TPU v7x, 32 devices: a whole 2x2x4 slice. The times are simulated.
32 devices in a mesh: fs: 16 (over z, y, x), tp: 2 (over core).
Axes of the slice: x: 2, y: 2, z: 4, core: 2. Of those that a mesh axis runs over, the one named last changes fastest.
Arguments:
- tokens: bfloat16 [6144, 2048], P('fs', 'tp'), may hold values from -8 to 8
- w_value: bfloat16 [2048, 1024], P('fs', 'tp'), may hold values from -0.125 to 0.125
- w_gate: bfloat16 [2048, 1024], P('fs', 'tp'), may hold values from -0.125 to 0.125
- conv_kernel: bfloat16 [31, 1024], replicated, may hold values from -1 to 1
- conv_gain: float32 [1024], replicated, may hold values from 0.1 to 1.9
- w_mix_out: bfloat16 [1024, 2048], P('fs', 'tp'), may hold values from -0.1875 to 0.1875
- mix_gain: float32 [2048], replicated, may hold values from 0.1 to 1.9
- w_up: bfloat16 [2048, 8192], P('fs', 'tp'), may hold values from -0.125 to 0.125
- w_down: bfloat16 [8192, 2048], P('tp', 'fs'), may hold values from -0.0625 to 0.0625
- out_gain: float32 [2048], replicated, may hold values from 0.1 to 1.9
Outputs:
- result: bfloat16 [6144, 2048], P('fs', 'tp')
All inputs are finite; a program needn't handle non-finite values.
Results may differ from a plain program's by a relative error of at most 0.013.
Values may be sent and summed in bfloat16 or wider, within the bound.
A program may use at most 128 MiB of HBM per device.

v0:
```python
import jax
import jax.numpy as jnp
from jax import lax
from jax.sharding import PartitionSpec as P

WIDTH = 2048
CHANNELS = 1024
KERNEL = 31
LENGTH = 128
norm_eps = 1e-05
residual_scale = 2.0**0.5


def causal_filter(gated, kernel):
    sequences = gated.shape[0] // LENGTH
    frames = gated.astype(jnp.float32).reshape(sequences, LENGTH, gated.shape[1])
    padded = jnp.pad(frames, ((0, 0), (KERNEL - 1, 0), (0, 0)))
    accumulated = jnp.zeros(frames.shape, jnp.float32)
    for offset in range(KERNEL):
        accumulated = (
            accumulated + kernel[offset].astype(jnp.float32) * padded[:, offset : offset + LENGTH]
        )
    return accumulated.reshape(gated.shape[0], gated.shape[1])


def normalize(values, total_sum, total_sq, entries, gain_vector):
    average = total_sum / entries
    spread = jnp.maximum(total_sq / entries - average * average, 0.0)
    return (values - average[:, None]) * lax.rsqrt(spread[:, None] + norm_eps) * gain_vector


def add_rows(piece, source):
    return jnp.dot(source, piece, preferred_element_type=jnp.float32)


def add_pair(pieces, source):
    first = jnp.dot(source, pieces[0], preferred_element_type=jnp.float32)
    second = jnp.dot(source, pieces[1], preferred_element_type=jnp.float32)
    return (first, second)


def per_device(
    tokens, w_value, w_gate, conv_kernel, conv_gain, w_mix_out, mix_gain, w_up, w_down, out_gain
):
    tp_rank = lax.axis_index("tp")
    width_part = tokens.shape[1]
    channel_part = w_value.shape[1]
    features = lax.all_gather(tokens, "tp", axis=1, tiled=True)
    values_proj, gate_proj = add_pair(
        (
            lax.all_gather(w_value, "fs", axis=0, tiled=True),
            lax.all_gather(w_gate, "fs", axis=0, tiled=True),
        ),
        source=features,
    )
    gated = (values_proj * jax.nn.sigmoid(gate_proj)).astype(jnp.bfloat16)
    kernel = lax.dynamic_slice_in_dim(conv_kernel, tp_rank * channel_part, channel_part, 1)
    filtered = causal_filter(gated, kernel)
    channel_sum, channel_sq = lax.psum(
        (jnp.sum(filtered, 1), jnp.sum(filtered * filtered, 1)), "tp"
    )
    channel_gain = lax.dynamic_slice_in_dim(conv_gain, tp_rank * channel_part, channel_part, 0)
    activated = jax.nn.silu(
        normalize(filtered, channel_sum, channel_sq, CHANNELS, channel_gain)
    ).astype(jnp.bfloat16)
    all_channels = lax.all_gather(activated, "tp", axis=1, tiled=True)
    mixed = add_rows(lax.all_gather(w_mix_out, "fs", axis=0, tiled=True), source=all_channels)
    combined = residual_scale * tokens.astype(jnp.float32) + mixed
    middle_sum, middle_sq = lax.psum((jnp.sum(combined, 1), jnp.sum(combined * combined, 1)), "tp")
    middle_gain = lax.dynamic_slice_in_dim(mix_gain, tp_rank * width_part, width_part, 0)
    middle = normalize(combined, middle_sum, middle_sq, WIDTH, middle_gain).astype(jnp.bfloat16)
    middle_whole = lax.all_gather(middle, "tp", axis=1, tiled=True)
    up_proj = add_rows(lax.all_gather(w_up, "fs", axis=0, tiled=True), source=middle_whole)
    hidden = jnp.square(jax.nn.relu(up_proj)).astype(jnp.bfloat16)
    terms = jnp.dot(
        hidden, lax.all_gather(w_down, "fs", axis=1, tiled=True), preferred_element_type=jnp.float32
    )
    down_sum = lax.psum_scatter(
        terms.astype(jnp.bfloat16), "tp", scatter_dimension=1, tiled=True
    ).astype(jnp.float32)
    final = residual_scale * middle.astype(jnp.float32) + down_sum
    final_sum, final_sq = lax.psum((jnp.sum(final, 1), jnp.sum(final * final, 1)), "tp")
    final_gain = lax.dynamic_slice_in_dim(out_gain, tp_rank * width_part, width_part, 0)
    return normalize(final, final_sum, final_sq, WIDTH, final_gain).astype(jnp.bfloat16)


def solution(mesh):
    in_specs = (
        P("fs", "tp"),
        P("fs", "tp"),
        P("fs", "tp"),
        P(),
        P(),
        P("fs", "tp"),
        P(),
        P("fs", "tp"),
        P("tp", "fs"),
        P(),
    )
    out_specs = P("fs", "tp")
    return jax.shard_map(
        per_device, mesh=mesh, in_specs=in_specs, out_specs=out_specs, check_vma=False
    )
```

profile of v0, /device:TPU:0, one launch (start us, length us, event | category | flops | bytes accessed | tf_op | source)
XLA Modules:
  0.0 715.3 jit_solution(9099667638542839668)
XLA Ops:
  6.5 0.0 all-gather.8.cloned.1.call-start
  6.5 0.7 all-gather.8.cloned.1.call-update
  7.3 0.0 all-gather.12.cloned.1.call-start
  7.3 0.7 all-gather.12.cloned.1.call-update
  8.0 0.0 all-gather.10.cloned.1.call-start
  8.1 0.7 all-gather.10.cloned.1.call-update
  8.7 0.0 all-gather.14.cloned.1.call-start
  8.8 0.5 all-gather.14.cloned.1.call-update
  9.3 0.0 all-gather.16.cloned.1.call-start
  9.4 0.8 dynamic_slice.13
  10.1 0.7 dynamic_slice.14
  10.8 1.2 dynamic-slice_convert_fusion.29
  12.0 1.2 dynamic-slice_convert_fusion.30
  13.2 8.2 %all-gather.8.cloned.1.call-done = bf16[384,2048]{1,0:T(8,128)(2,1)} async-done(((bf16[384,1024]{1,0:T(8,128)(2,1)}), bf16[384,2048]{1,0:T(8,128)(2,1)}) %all-gather.8.cloned.1.call-update) | async-done | bytes 1572880 | tf_op jit(solution)/shard_map/all_gather | solution.py:48
  21.4 0.0 copy-start.2
  21.4 64.4 %all-gather.12.cloned.1.call-done = bf16[2048,512]{1,0:T(8,128)(2,1)} async-done(((bf16[128,512]{1,0:T(8,128)(2,1)}), bf16[2048,512]{1,0:T(8,128)(2,1)}) %all-gather.12.cloned.1.call-update) | async-done | bytes 2097168 | tf_op jit(solution)/shard_map/all_gather | solution.py:52
  85.8 3.2 fusion.5
  88.9 58.8 %all-gather.10.cloned.1.call-done = bf16[2048,512]{1,0:T(8,128)(2,1)} async-done(((bf16[128,512]{1,0:T(8,128)(2,1)}), bf16[2048,512]{1,0:T(8,128)(2,1)}) %all-gather.10.cloned.1.call-update) | async-done | bytes 2097168 | tf_op jit(solution)/shard_map/all_gather | solution.py:51
  147.8 0.0 copy-done.2
  147.8 2.6 fusion.6
  150.3 0.1 convert.32
  150.4 3.5 fusion.72
  154.0 0.0 copy-start.1
  154.0 2.6 all-reduce.3
  156.6 0.3 multiply_convert_fusion.3
  156.9 2.4 all_gather.27
  159.3 50.3 %all-gather.14.cloned.1.call-done = bf16[1024,1024]{1,0:T(8,128)(2,1)} async-done(((bf16[64,1024]{1,0:T(8,128)(2,1)}), bf16[1024,1024]{1,0:T(8,128)(2,1)}) %all-gather.14.cloned.1.call-update) | async-done | bytes 2097168 | tf_op jit(solution)/shard_map/all_gather | solution.py:67
  209.6 0.0 copy-done.1
  209.6 2.8 fusion.71
  212.4 2.5 all-reduce.2
  214.9 1.2 multiply_convert_fusion.2
  216.0 0.0 all-gather.16.cloned.1.call-update
  216.0 0.0 all-gather.18.cloned.1.call-start
  216.1 0.5 all-gather.18.cloned.1.call-update
  216.6 0.0 all-gather.20.cloned.1.call-start
  216.7 0.7 all-gather.20.cloned.1.call-update
  217.4 0.2 reduce-scatter.2.cloned.1.call-start
  217.6 7.2 %all-gather.16.cloned.1.call-done = bf16[384,2048]{1,0:T(8,128)(2,1)} async-done(((bf16[384,1024]{1,0:T(8,128)(2,1)}), bf16[384,2048]{1,0:T(8,128)(2,1)}) %all-gather.16.cloned.1.call-update) | async-done | bytes 1572880 | tf_op jit(solution)/shard_map/all_gather | solution.py:72
  224.8 194.8 %all-gather.18.cloned.1.call-done = bf16[2048,4096]{1,0:T(8,128)(2,1)} async-done(((bf16[128,4096]{1,0:T(8,128)(2,1)}), bf16[2048,4096]{1,0:T(8,128)(2,1)}) %all-gather.18.cloned.1.call-update) | async-done | bytes 16777232 | tf_op jit(solution)/shard_map/all_gather | solution.py:73
  419.6 250.0 %all-gather.20.cloned.1.call-done = bf16[4096,2048]{1,0:T(8,128)(2,1)} async-done(((bf16[4096,128]{1,0:T(8,128)(2,1)}), bf16[4096,2048]{1,0:T(8,128)(2,1)}) %all-gather.20.cloned.1.call-update) | async-done | bytes 16777232 | tf_op jit(solution)/shard_map/all_gather | solution.py:76
  669.6 25.3 %fusion.2 = bf16[384,2048]{1,0:T(8,128)(2,1)} fusion(bf16[4096,2048]{1,0:T(8,128)(2,1)} %all-gather.20.cloned.1.call-done, bf16[384,2048]{1,0:T(8,128)(2,1)} %all-gather.16.cloned.1.call-done, bf16[2048,4096]{1,0:T(8,128)(2,1)} %all-gather.18.cloned.1.call-done), kind=kOutput, calls=%fused_computation.3 | convolution fusion | flops 12890406912 | bytes 36700160 | tf_op jit(solution)/shard_map/dot_general | solution.py:75
  694.9 0.0 reduce-scatter.2.cloned.1.call-update
  694.9 0.0 dynamic-slice-start
  695.0 7.3 %reduce-scatter.2.cloned.1.call-done = bf16[384,1024]{1,0:T(8,128)(2,1)} async-done(((bf16[384,2048]{1,0:T(8,128)(2,1)}), bf16[384,1024]{1,0:T(8,128)(2,1)}) %reduce-scatter.2.cloned.1.call-update) | async-done | bytes 786448 | tf_op jit(solution)/shard_map/reduce_scatter | solution.py:78
  702.2 0.0 copy-start
  702.2 1.9 fusion.7
  704.1 2.5 all-reduce.1
  706.6 0.0 dynamic-slice-done
  706.6 0.0 copy-done
  706.6 1.9 multiply_convert_fusion.1
  (3 shorter events, 0.0 us)
Async XLA Ops:
  6.5 14.9 %all-gather.8.cloned.1.call-start = ((), (), s32[]{:S(2)}) async-start(), calls=%async_computation.1 | async-start | bytes 2359296 | tf_op jit(solution)/shard_map/all_gather | solution.py:48
  7.3 78.5 %all-gather.12.cloned.1.call-start = ((), (), s32[]{:S(2)}) async-start(), calls=%async_computation.3 | async-start | bytes 2228224 | tf_op jit(solution)/shard_map/all_gather | solution.py:52
  8.0 139.8 %all-gather.10.cloned.1.call-start = ((), (), s32[]{:S(2)}) async-start(), calls=%async_computation.2 | async-start | bytes 2228224 | tf_op jit(solution)/shard_map/all_gather | solution.py:51
  8.7 200.9 %all-gather.14.cloned.1.call-start = ((), (), s32[]{:S(2)}) async-start(), calls=%async_computation.4 | async-start | bytes 2228224 | tf_op jit(solution)/shard_map/all_gather | solution.py:67
  9.3 215.5 %all-gather.16.cloned.1.call-start = ((), (), s32[]{:S(2)}) async-start(), calls=%async_computation.5 | async-start | bytes 2359296 | tf_op jit(solution)/shard_map/all_gather | solution.py:72
  21.4 126.3 %copy-start.2 = (bf16[384,2048]{1,0:T(8,128)(2,1)S(1)}, bf16[384,2048]{1,0:T(8,128)(2,1)}, u32[]{:S(2)}) copy-start(bf16[384,2048]{1,0:T(8,128)(2,1)} %all-gather.8.cloned.1.call-done) | copy-start | bytes 4718596
  154.0 55.6 %copy-start.1 = (bf16[384,1024]{1,0:T(8,128)(2,1)S(1)}, bf16[384,1024]{1,0:T(8,128)(2,1)}, u32[]{:S(2)}) copy-start(bf16[384,1024]{1,0:T(8,128)(2,1)} %param.10) | copy-start | bytes 2359300
  216.0 203.6 %all-gather.18.cloned.1.call-start = ((), (), s32[]{:S(2)}) async-start(), calls=%async_computation.6 | async-start | bytes 17825792 | tf_op jit(solution)/shard_map/all_gather | solution.py:73
  216.6 453.0 %all-gather.20.cloned.1.call-start = ((), (), s32[]{:S(2)}) async-start(), calls=%async_computation.7 | async-start | bytes 17825792 | tf_op jit(solution)/shard_map/all_gather | solution.py:76
  217.4 484.9 %reduce-scatter.2.cloned.1.call-start = ((), (), s32[]{:S(2)}) async-start(), calls=%async_computation.8 | async-start | bytes 2359296 | tf_op jit(solution)/shard_map/reduce_scatter | solution.py:78
  694.9 11.6 %dynamic-slice-start = ((f32[2048]{0:T(1024)}, s32[]{:T(128)}), f32[1024]{0:T(1024)S(1)}, s32[]{:S(2)}) async-start(f32[2048]{0:T(1024)} %param.19, s32[]{:T(128)} %select_n.9), calls=%async_computation.9 | async-start | bytes 8704 | tf_op jit(solution)/shard_map/dynamic_slice | solution.py:83
  702.2 4.3 copy-start
Sparse Core Ops, SparseCore 0:
  8.9 12.5 all-gather.7
  24.2 61.5 all-gather.11
  88.6 59.1 all-gather.9
  150.4 59.1 all-gather.13
  216.2 8.5 all-gather.15
  227.4 192.1 all-gather.17
  422.3 247.2 all-gather.19
  695.1 7.1 reduce-scatter.1
where the time goes:
time: 716 us; the launch traced here: 715 us
  waiting for transfers between devices  645 us (90%)
  matrix products  33.7 us (5%)
  between operations  13.6 us (2%)
  other arithmetic  11.3 us (2%)
  blocking collectives  9.91 us (1%)
    all_gather x1, waiting for transfers between devices, per_device(): lax.all_gather(w_down, 'fs', axis=1, tiled=True)  250 us
    all_gather x1, waiting for transfers between devices, per_device(): lax.all_gather(w_up, 'fs', axis=0, tiled=True)  195 us
    all_gather x1, waiting for transfers between devices, per_device(): lax.all_gather(w_gate, 'fs', axis=0, tiled=True)  64.4 us
    all_gather x1, waiting for transfers between devices, per_device(): lax.all_gather(w_value, 'fs', axis=0, tiled=True)  58.8 us
    all_gather x1, waiting for transfers between devices, per_device(): lax.all_gather(w_mix_out, 'fs', axis=0, tiled=True)  50.3 us
    dot_general x1, matrix products, per_device(): jnp.dot(hidden, lax.all_gather(w_down, 'fs', axis=1, tiled=True), preferr...  25.3 us
  transfers between devices with their start and end apart: 8, of which 8 were waited for; matrix products, arithmetic and copies ran while one was open for 2% of the time, Pallas kernels for 0%

commit v1 on v0

--- a/solution.py
+++ b/solution.py
@@ -73,7 +73,9 @@
     up_proj = add_rows(lax.all_gather(w_up, "fs", axis=0, tiled=True), source=middle_whole)
     hidden = jnp.square(jax.nn.relu(up_proj)).astype(jnp.bfloat16)
     terms = jnp.dot(
-        hidden, lax.all_gather(w_down, "fs", axis=1, tiled=True), preferred_element_type=jnp.float32
+        hidden,
+        jnp.concatenate(lax.all_gather(w_down, "fs"), axis=1),
+        preferred_element_type=jnp.float32,
     )
     down_sum = lax.psum_scatter(
         terms.astype(jnp.bfloat16), "tp", scatter_dimension=1, tiled=True

time: 716 us -> 647 us (0.904)
  waiting for transfers between devices: 645 us -> 564 us
  local copies, waits for them, and re-layouts: 1.48 us -> 21.7 us
    all_gather x1, waiting for transfers between devices: 250 us -> 185 us  [per_device(): lax.all_gather(w_down, 'fs')]
    reshape x0 -> x1, local copies, waits for them, and re-layouts: none -> 21.6 us  [per_device(): jnp.concatenate(lax.all_gather(w_down, 'fs'), axis=1)]
    all_gather x1, waiting for transfers between devices: 195 us -> 183 us  [per_device(): lax.all_gather(w_up, 'fs', axis=0, tiled=True)]
    all_gather x1, waiting for transfers between devices: 7.2 us -> 0.01 us  [per_device(): middle_whole = lax.all_gather(middle, 'tp', axis=1, tiled=True)]
  transfers between devices with their start and end apart: 8 -> 8, of which waited for: 8 -> 7; matrix products, arithmetic and copies ran while one was open for 2% -> 6% of each run, Pallas kernels for 0% -> 0%
where the time goes in v1:
time: 647 us; the launch traced here: 646 us
  waiting for transfers between devices  564 us (87%)
  matrix products  27.5 us (4%)
  local copies, waits for them, and re-layouts  21.7 us (3%)
  between operations  13.6 us (2%)
  blocking collectives  9.91 us (2%)
  other arithmetic  9.18 us (1%)
    all_gather x1, waiting for transfers between devices, per_device(): lax.all_gather(w_down, 'fs')  185 us
    all_gather x1, waiting for transfers between devices, per_device(): lax.all_gather(w_up, 'fs', axis=0, tiled=True)  183 us
    all_gather x1, waiting for transfers between devices, per_device(): lax.all_gather(w_gate, 'fs', axis=0, tiled=True)  64.4 us
    all_gather x1, waiting for transfers between devices, per_device(): lax.all_gather(w_value, 'fs', axis=0, tiled=True)  58.8 us
    all_gather x1, waiting for transfers between devices, per_device(): lax.all_gather(w_mix_out, 'fs', axis=0, tiled=True)  50.3 us
    reshape x1, local copies, waits for them, and re-layouts, per_device(): jnp.concatenate(lax.all_gather(w_down, 'fs'), axis=1)  21.6 us
    dot_general x1, matrix products, per_device(): jnp.dot(hidden, jnp.concatenate(lax.all_gather(w_down, 'fs'), axis=1), pr...  19 us
  transfers between devices with their start and end apart: 8, of which 7 were waited for; matrix products, arithmetic and copies ran while one was open for 6% of the time, Pallas kernels for 0%

profile of v1, /device:TPU:0, one launch (start us, length us, event | category | flops | bytes accessed | tf_op | source)
XLA Modules:
  0.0 645.9 jit_solution(10999383407543221845)
XLA Ops:
  6.5 0.0 copy-start.4
  6.5 0.0 copy-start.3
  6.5 0.0 copy-start.2
  6.5 0.0 all-gather.9.cloned.1.call-start
  6.5 0.7 all-gather.9.cloned.1.call-update
  7.3 0.0 all-gather.13.cloned.1.call-start
  7.3 0.7 all-gather.13.cloned.1.call-update
  8.0 0.0 all-gather.11.cloned.1.call-start
  8.1 0.7 all-gather.11.cloned.1.call-update
  8.7 0.0 all-gather.15.cloned.1.call-start
  8.8 0.5 all-gather.15.cloned.1.call-update
  9.3 0.0 all-gather.21.cloned.1.call-start
  9.4 0.5 all-gather.21.cloned.1.call-update
  9.9 0.0 all-gather.17.cloned.1.call-start
  10.0 0.0 copy-done.4
  10.0 0.1 dynamic_slice.13
  10.1 0.0 copy-done.3
  10.1 0.0 copy-done.2
  10.1 0.1 dynamic-slice_convert_fusion.29
  10.2 0.2 dynamic-slice_convert_fusion.30
  10.4 11.1 %all-gather.9.cloned.1.call-done = bf16[384,2048]{1,0:T(8,128)(2,1)} async-done(((bf16[384,1024]{1,0:T(8,128)(2,1)}), bf16[384,2048]{1,0:T(8,128)(2,1)}) %all-gather.9.cloned.1.call-update) | async-done | bytes 1572880 | tf_op jit(solution)/shard_map/all_gather | solution.py:48
  21.4 0.0 copy-start.5
  21.4 64.4 %all-gather.13.cloned.1.call-done = bf16[2048,512]{1,0:T(8,128)(2,1)} async-done(((bf16[128,512]{1,0:T(8,128)(2,1)}), bf16[2048,512]{1,0:T(8,128)(2,1)}) %all-gather.13.cloned.1.call-update) | async-done | bytes 2097168 | tf_op jit(solution)/shard_map/all_gather | solution.py:52
  85.8 3.2 fusion.4
  89.0 58.8 %all-gather.11.cloned.1.call-done = bf16[2048,512]{1,0:T(8,128)(2,1)} async-done(((bf16[128,512]{1,0:T(8,128)(2,1)}), bf16[2048,512]{1,0:T(8,128)(2,1)}) %all-gather.11.cloned.1.call-update) | async-done | bytes 2097168 | tf_op jit(solution)/shard_map/all_gather | solution.py:51
  147.8 0.0 copy-done.5
  147.8 2.6 fusion.5
  150.3 0.1 convert.32
  150.4 3.5 fusion.71
  154.0 0.0 copy-start.1
  154.0 2.6 all-reduce.3
  156.6 0.3 multiply_convert_fusion.3
  156.9 2.4 all_gather.30
  159.3 50.3 %all-gather.15.cloned.1.call-done = bf16[1024,1024]{1,0:T(8,128)(2,1)} async-done(((bf16[64,1024]{1,0:T(8,128)(2,1)}), bf16[1024,1024]{1,0:T(8,128)(2,1)}) %all-gather.15.cloned.1.call-update) | async-done | bytes 2097168 | tf_op jit(solution)/shard_map/all_gather | solution.py:67
  209.6 0.0 copy-done.1
  209.6 2.8 fusion.70
  212.4 2.5 all-reduce.2
  214.9 1.2 multiply_convert_fusion.2
  216.0 0.0 all-gather.17.cloned.1.call-update
  216.0 0.0 all-gather.19.cloned.1.call-start
  216.1 0.7 all-gather.19.cloned.1.call-update
  216.8 0.0 reduce-scatter.2.cloned.1.call-start
  216.8 185.2 %all-gather.21.cloned.1.call-done = bf16[65536,128]{1,0:T(8,128)(2,1)} async-done(((bf16[4096,128]{1,0:T(8,128)(2,1)}), bf16[65536,128]{1,0:T(8,128)(2,1)}) %all-gather.21.cloned.1.call-update) | async-done | bytes 16777232 | tf_op jit(solution)/shard_map/all_gather | solution.py:77
  402.1 21.6 %copy.11 = bf16[4096,16,128]{0,2,1:T(8,128)(2,1)} copy(bf16[4096,16,128]{2,0,1:T(8,128)(2,1)} %bitcast.56) | data formatting | bytes 33554432 | tf_op jit(solution)/shard_map/reshape | solution.py:77
  423.6 0.0 all-gather.17.cloned.1.call-done
  423.6 182.8 %all-gather.19.cloned.1.call-done = bf16[2048,4096]{1,0:T(8,128)(2,1)} async-done(((bf16[128,4096]{1,0:T(8,128)(2,1)}), bf16[2048,4096]{1,0:T(8,128)(2,1)}) %all-gather.19.cloned.1.call-update) | async-done | bytes 16777232 | tf_op jit(solution)/shard_map/all_gather | solution.py:73
  606.5 19.0 %fusion.1 = bf16[384,2048]{1,0:T(8,128)(2,1)} fusion(bf16[4096,2048]{0,1:T(8,128)(2,1)} %bitcast.57, bf16[384,2048]{1,0:T(8,128)(2,1)} %all-gather.17.cloned.1.call-done, bf16[2048,4096]{1,0:T(8,128)(2,1)} %all-gather.19.cloned.1.call-done), kind=kOutput, calls=%fused_computation.2 | convolution fusion | flops 12890406912 | bytes 36700160 | tf_op jit(solution)/shard_map/dot_general | solution.py:75
  625.5 0.0 reduce-scatter.2.cloned.1.call-update
  625.5 0.0 dynamic-slice-start
  625.5 7.3 %reduce-scatter.2.cloned.1.call-done = bf16[384,1024]{1,0:T(8,128)(2,1)} async-done(((bf16[384,2048]{1,0:T(8,128)(2,1)}), bf16[384,1024]{1,0:T(8,128)(2,1)}) %reduce-scatter.2.cloned.1.call-update) | async-done | bytes 786448 | tf_op jit(solution)/shard_map/reduce_scatter | solution.py:80
  632.8 0.0 copy-start
  632.8 1.9 fusion.6
  634.7 2.5 all-reduce.1
  637.1 0.0 dynamic-slice-done
  637.1 0.0 copy-done
  637.1 1.9 multiply_convert_fusion.1
  (4 shorter events, 0.0 us)
Async XLA Ops:
  6.5 3.4 copy-start.4
  6.5 3.5 copy-start.3
  6.5 3.5 copy-start.2
  6.5 14.9 %all-gather.9.cloned.1.call-start = ((), (), s32[]{:S(2)}) async-start(), calls=%async_computation.1 | async-start | bytes 2359296 | tf_op jit(solution)/shard_map/all_gather | solution.py:48
  7.3 78.5 %all-gather.13.cloned.1.call-start = ((), (), s32[]{:S(2)}) async-start(), calls=%async_computation.3 | async-start | bytes 2228224 | tf_op jit(solution)/shard_map/all_gather | solution.py:52
  8.0 139.8 %all-gather.11.cloned.1.call-start = ((), (), s32[]{:S(2)}) async-start(), calls=%async_computation.2 | async-start | bytes 2228224 | tf_op jit(solution)/shard_map/all_gather | solution.py:51
  8.7 200.9 %all-gather.15.cloned.1.call-start = ((), (), s32[]{:S(2)}) async-start(), calls=%async_computation.4 | async-start | bytes 2228224 | tf_op jit(solution)/shard_map/all_gather | solution.py:67
  9.3 392.7 %all-gather.21.cloned.1.call-start = ((), (), s32[]{:S(2)}) async-start(), calls=%async_computation.8 | async-start | bytes 17825792 | tf_op jit(solution)/shard_map/all_gather | solution.py:77
  9.9 413.7 %all-gather.17.cloned.1.call-start = ((), (), s32[]{:S(2)}) async-start(), calls=%async_computation.5 | async-start | bytes 2359296 | tf_op jit(solution)/shard_map/all_gather | solution.py:72
  21.4 126.3 %copy-start.5 = (bf16[384,2048]{1,0:T(8,128)(2,1)S(1)}, bf16[384,2048]{1,0:T(8,128)(2,1)}, u32[]{:S(2)}) copy-start(bf16[384,2048]{1,0:T(8,128)(2,1)} %all-gather.9.cloned.1.call-done) | copy-start | bytes 4718596
  154.0 55.6 %copy-start.1 = (bf16[384,1024]{1,0:T(8,128)(2,1)S(1)}, bf16[384,1024]{1,0:T(8,128)(2,1)}, u32[]{:S(2)}) copy-start(bf16[384,1024]{1,0:T(8,128)(2,1)} %param.10) | copy-start | bytes 2359300
  216.0 390.4 %all-gather.19.cloned.1.call-start = ((), (), s32[]{:S(2)}) async-start(), calls=%async_computation.6 | async-start | bytes 17825792 | tf_op jit(solution)/shard_map/all_gather | solution.py:73
  216.8 416.0 %reduce-scatter.2.cloned.1.call-start = ((), (), s32[]{:S(2)}) async-start(), calls=%async_computation.7 | async-start | bytes 2359296 | tf_op jit(solution)/shard_map/reduce_scatter | solution.py:80
  625.5 11.6 %dynamic-slice-start = ((f32[2048]{0:T(1024)}, s32[]{:T(128)}), f32[1024]{0:T(1024)S(1)}, s32[]{:S(2)}) async-start(f32[2048]{0:T(1024)} %param.19, s32[]{:T(128)} %select_n.9), calls=%async_computation.9 | async-start | bytes 8704 | tf_op jit(solution)/shard_map/dynamic_slice | solution.py:85
  632.8 4.3 copy-start
Sparse Core Ops, SparseCore 0:
  8.9 12.5 all-gather.8
  24.2 61.5 all-gather.12
  88.6 59.1 all-gather.10
  150.4 59.1 all-gather.14
  212.2 189.7 all-gather.20
  403.5 7.9 all-gather.16
  414.2 192.1 all-gather.18
  625.6 7.1 reduce-scatter.1
